TPU v7x, 32 devices: a whole 2x2x4 slice. The times are simulated.
32 devices in a mesh: sp: 16 (over z, y, x), tp: 2 (over core).
Axes of the slice: x: 2, y: 2, z: 4, core: 2. Of those that a mesh axis runs over, the one named last changes fastest.
Arguments:
- pool_input: bfloat16 [8192, 512], P('sp', 'tp'), may hold values from -8 to 8
- documents: int32 [8192], P('sp'), may hold values from 0 to 3, never falling along the last dimension, each value on 1 to 4096 neighbouring positions
- residual: bfloat16 [8192, 2048], P(('sp', 'tp')), may hold values from -6 to 6
- group_weights: bfloat16 [8, 64, 64], replicated, may hold values from -0.75 to 0.75
- pool_gain: bfloat16 [512], replicated, may hold values from 0.099609375 to 1.8984375
- output_weight: bfloat16 [512, 2048], replicated, may hold values from -0.25 to 0.25
- mixer_gain: bfloat16 [2048], replicated, may hold values from 0.099609375 to 1.8984375
- routed_gain: bfloat16 [2048], replicated, may hold values from 0.099609375 to 1.8984375
- final_gain: bfloat16 [2048], replicated, may hold values from 0.099609375 to 1.8984375
- chosen_group: int32 [8192, 1], P(('sp', 'tp')), may hold values from 0 to 15; in each aligned block of 256 rows (0 to 255, 256 to 511, ...) at most 32 rows name the same one
- chosen_experts: int32 [8192, 2], P(('sp', 'tp')), may hold values from 0 to 2, all different within a row
- expert_share: bfloat16 [8192, 2], P(('sp', 'tp')), may hold values from 0.099609375 to 1
- expert_gate: bfloat16 [48, 2048, 1024], P('sp', None, 'tp'), may hold values from -0.125 to 0.125
- expert_up: bfloat16 [48, 2048, 1024], P('sp', None, 'tp'), may hold values from -0.125 to 0.125
- expert_down: bfloat16 [48, 1024, 2048], P('sp', 'tp'), may hold values from -0.1875 to 0.1875
Outputs:
- updated: bfloat16 [8192, 2048], P(('sp', 'tp'))
Inputs may be any that keep to these rules, and one draw needn't show every extreme that they name: `documents`: document numbers never fall along the sequence; every number appears, and a document holds 1 to 4096 positions. `chosen_group`: among the rows of one device at most 32 name the same group, and in every draw some group is named by exactly 32 rows of some device. `chosen_experts`: each row names 2 different experts of its group.
All inputs are finite; a program needn't handle non-finite values.
Results may differ from a plain program's by a relative error of at most 0.012.
Values may be sent and summed in bfloat16 or wider, within the bound.
A program may use at most 128 MiB of HBM per device.

v0:
```python
import functools

import jax
import jax.numpy as jnp
from jax import lax
from jax.experimental import pallas as pl
from jax.experimental.pallas import tpu as pltpu
from jax.sharding import PartitionSpec as P

EPSILON = 1e-06


PHASES = 4
LANES = 128


def greet():
    barrier = pltpu.get_barrier_semaphore()
    count = lax.axis_size("sp")
    me = lax.axis_index("sp")

    def signal(step, carry):
        pl.semaphore_signal(barrier, inc=1, device_id={"sp": lax.rem(me + step, count)})
        return carry

    lax.fori_loop(1, count, signal, 0)
    pl.semaphore_signal(barrier, inc=1, device_id={"tp": 1 - lax.axis_index("tp")})


def settle(ref, sem):
    pltpu.make_async_copy(ref, ref, sem).wait()


def other_plane(plane, phase):
    turn = PHASES - 1 - phase
    high = lax.rem(plane // 2 + turn // 2, 2)
    low = lax.rem(plane + turn, 2)
    return high * 2 + low


def mixer_stage(
    count,
    docs,
    me,
    tp_rank,
    pool_ref,
    docs_ref,
    weights_ref,
    pool_gain_ref,
    padded,
    edge_docs,
    table,
    tables,
    pooled,
    edge_send,
    edge_recv,
    table_send,
    table_recv,
    spread,
):
    length, part = pool_ref.shape
    reach = length // 2
    barrier = pltpu.get_barrier_semaphore()
    own_rows = pltpu.make_async_copy(pool_ref, padded.at[pl.ds(reach, length)], edge_recv.at[4])
    own_rows.start()
    own_docs = jnp.concatenate([docs_ref[0], docs_ref[1]], axis=1).astype(jnp.float32)
    deep = table.shape[0]
    hot = (
        lax.broadcasted_iota(jnp.int32, (deep, length), 0).astype(jnp.float32) == own_docs
    ).astype(jnp.float32)
    table[:, :part] = jnp.dot(
        hot.astype(jnp.bfloat16), pool_ref[...], preferred_element_type=jnp.float32
    )
    table[:, part:] = jnp.broadcast_to(jnp.sum(hot, axis=1, keepdims=True), (deep, LANES))
    local_copy = pltpu.make_async_copy(table, tables.at[me], table_recv.at[me])
    local_copy.start()
    pl.semaphore_wait(barrier, count)
    right, left = lax.rem(me + 1, count), lax.rem(me + count - 1, count)
    copies = []
    for side, (start, target) in enumerate(((reach, right), (0, left))):
        copies.append(
            pltpu.make_async_remote_copy(
                pool_ref.at[pl.ds(start, reach)],
                padded.at[pl.ds(side * (length + reach), reach)],
                edge_send.at[side],
                edge_recv.at[side],
                device_id={"sp": target},
            )
        )
        copies.append(
            pltpu.make_async_remote_copy(
                docs_ref.at[1 - side],
                edge_docs.at[side],
                edge_send.at[2 + side],
                edge_recv.at[2 + side],
                device_id={"sp": target},
            )
        )

    def table_copy(step):
        return pltpu.make_async_remote_copy(
            table,
            tables.at[me],
            table_send.at[step],
            table_recv.at[me],
            device_id={"sp": lax.rem(me + step, count)},
        )

    for copy in copies:
        copy.start()

    def start_table(step, carry):
        table_copy(step).start()
        return carry

    lax.fori_loop(1, count, start_table, 0)
    spread()

    local_groups = part // weights_ref.shape[1]
    group_dim = weights_ref.shape[1]
    bands = []
    for group in range(local_groups):
        own = weights_ref[tp_rank * local_groups + group]
        pieces = [jnp.zeros_like(own)] * local_groups
        pieces[group] = own
        bands.append(jnp.concatenate(pieces, axis=1))
    block_weight = jnp.concatenate(bands, axis=0)
    all_gain = pool_gain_ref[...].astype(jnp.float32).reshape(1, -1)
    gain = all_gain[:, :part]
    for other in range(1, all_gain.shape[1] // part):
        rest = all_gain[:, other * part : (other + 1) * part]
        gain = jnp.where(tp_rank == other, rest, gain)
    own_column = jnp.transpose(jnp.broadcast_to(own_docs, (LANES, length)))[:, :1]
    block = length // 4
    span = block + 2 * reach
    offsets = (
        lax.broadcasted_iota(jnp.int32, (block, span), 1)
        - reach
        - lax.broadcasted_iota(jnp.int32, (block, span), 0)
    )
    levels = lax.rem(lax.broadcasted_iota(jnp.int32, (block, part), 1) // group_dim, 4)
    own_rows.wait()
    for copy in copies:
        copy.wait()
    before = jnp.where(me == 0, -1.0, edge_docs[0].astype(jnp.float32))
    after = jnp.where(me == count - 1, -1.0, edge_docs[1].astype(jnp.float32))
    all_docs = jnp.concatenate([before, own_docs, after], axis=1)

    def end_table(step, carry):
        settle(tables.at[step], table_recv.at[step])
        return carry

    lax.fori_loop(0, count, end_table, 0)
    totals = jnp.sum(tables[...], axis=0)
    doc_means = totals[:, :part] / totals[:, part : part + 1]
    for index in range(length // block):
        rows = slice(index * block, (index + 1) * block)
        reached = slice(index * block, index * block + span)
        column = own_column[rows]
        same = all_docs[:, reached] == column
        values = padded[reached]
        mean = jnp.zeros((block, part), jnp.float32)
        for doc in range(docs):
            mean = jnp.where(column == doc, doc_means[doc : doc + 1], mean)
        for level in range(3):
            half_width = length * (1 << level) // 8
            inside = same & (offsets >= -half_width) & (offsets < half_width)
            mask = jnp.where(inside, 1.0, 0.0)
            sums = jnp.dot(
                mask.astype(jnp.bfloat16), values, preferred_element_type=jnp.float32
            )
            sizes = jnp.sum(mask, axis=1, keepdims=True)
            mean = jnp.where(levels == level, sums / sizes, mean)
        difference = (mean - pool_ref[rows].astype(jnp.float32)).astype(jnp.bfloat16)
        pooled[rows] = (
            jnp.dot(difference, block_weight, preferred_element_type=jnp.float32) * gain
        ).astype(jnp.bfloat16)

    def sent_table(step, carry):
        table_copy(step).wait_send()
        return carry

    lax.fori_loop(1, count, sent_table, 0)


def route(group_ref, experts_ref, share_ref, cap, slots, pick, share_send):
    rows = group_ref.shape[1]
    ids = group_ref[...]
    names = lax.broadcasted_iota(jnp.int32, (LANES, rows), 0)
    member = (ids == names).astype(jnp.float32)
    earlier = (
        lax.broadcasted_iota(jnp.int32, (rows, rows), 0)
        < lax.broadcasted_iota(jnp.int32, (rows, rows), 1)
    ).astype(jnp.float32)
    ahead = jnp.dot(
        member.astype(jnp.bfloat16),
        earlier.astype(jnp.bfloat16),
        preferred_element_type=jnp.float32,
    )
    rank = jnp.sum(ahead * member, axis=0, keepdims=True)
    slot = ids.astype(jnp.float32) * cap + rank
    chosen = (
        slot == lax.broadcasted_iota(jnp.int32, (slots, rows), 0).astype(jnp.float32)
    ).astype(jnp.float32)
    pick[...] = jnp.transpose(chosen).astype(jnp.bfloat16)
    placing = chosen.astype(jnp.bfloat16)
    total = jnp.zeros((LANES, rows), jnp.float32)
    for nth in range(experts_ref.shape[0]):
        named = experts_ref[nth : nth + 1] == names
        total = total + jnp.where(named, share_ref[nth : nth + 1].astype(jnp.float32), 0.0)
    shares = jnp.transpose(total).astype(jnp.bfloat16)
    share_send[...] = jnp.dot(placing, shares, preferred_element_type=jnp.float32).astype(
        jnp.bfloat16
    )
    return placing


def scaled(values, gain):
    return values * lax.rsqrt(jnp.mean(values * values, axis=-1, keepdims=True) + EPSILON) * gain


def layer_kernel(
    count,
    docs,
    pool_ref,
    docs_ref,
    residual_hbm,
    weights_ref,
    pool_gain_ref,
    output_hbm,
    mixer_gain_ref,
    routed_gain_ref,
    final_gain_ref,
    group_ref,
    experts_ref,
    share_ref,
    gate_hbm,
    up_hbm,
    down_hbm,
    out_ref,
    padded,
    edge_docs,
    table,
    tables,
    pooled,
    swapped,
    output_weight,
    residual,
    mixed,
    stream,
    wide,
    pick,
    share_send,
    arrived_share,
    send_ref,
    fetched,
    arrived,
    gates,
    ups,
    downs,
    hidden,
    kept,
    outgoing,
    incoming,
    result,
    edge_send,
    edge_recv,
    table_send,
    table_recv,
    swap_sem,
    spread_send,
    spread_recv,
    weight_sem,
    send_sem,
    recv_sem,
    forward_send,
    forward_recv,
    part_send,
    part_recv,
    back_send,
    back_recv,
):
    me, tp_rank = lax.axis_index("sp"), lax.axis_index("tp")
    per = count // PHASES
    plane, place = me // per, lax.rem(me, per)
    rows, width = out_ref.shape
    slots = send_ref.shape[0]
    cap = slots // count
    experts, _, units = gates.shape
    half = per * cap
    part = pool_ref.shape[1]
    greet()

    def block(index):
        return pl.ds(pl.multiple_of(index * cap, cap), cap)

    def target(step):
        phase = step // per
        spot = lax.rem(step + place, per)
        return phase, spot, other_plane(plane, phase) * per + spot

    early = [
        pltpu.make_async_copy(output_hbm, output_weight, weight_sem.at[3]),
        pltpu.make_async_copy(residual_hbm, residual, weight_sem.at[4]),
    ]
    loads = [
        pltpu.make_async_copy(gate_hbm, gates, weight_sem.at[0]),
        pltpu.make_async_copy(up_hbm, ups, weight_sem.at[1]),
        pltpu.make_async_copy(down_hbm, downs, weight_sem.at[2]),
    ]
    for load in early + loads:
        load.start()
    placing = route(group_ref, experts_ref, share_ref, cap, slots, pick, share_send)

    def share_copy(step):
        phase, _, dest = target(step)
        return dest, pltpu.make_async_remote_copy(
            share_send.at[block(dest)],
            arrived_share.at[phase, block(place)],
            spread_send.at[step],
            spread_recv.at[phase * per + place],
            device_id={"sp": dest},
        )

    def spread():
        pltpu.make_async_copy(
            share_send.at[block(me)],
            arrived_share.at[PHASES - 1, block(place)],
            spread_recv.at[(PHASES - 1) * per + place],
        ).start()

        def start_share(step, carry):
            dest, copy = share_copy(step)

            @pl.when(dest != me)
            def _():
                copy.start()

            return carry

        lax.fori_loop(0, count, start_share, 0)

    mixer_stage(
        count,
        docs,
        me,
        tp_rank,
        pool_ref,
        docs_ref,
        weights_ref,
        pool_gain_ref,
        padded,
        edge_docs,
        table,
        tables,
        pooled,
        edge_send,
        edge_recv,
        table_send,
        table_recv,
        spread,
    )
    trade = pltpu.make_async_remote_copy(
        pooled.at[pl.ds(pl.multiple_of((1 - tp_rank) * rows, rows), rows)],
        swapped,
        swap_sem.at[0],
        swap_sem.at[1],
        device_id={"tp": 1 - tp_rank},
    )
    trade.start()
    for load in early:
        load.wait()
    own_part = pooled[pl.ds(pl.multiple_of(tp_rank * rows, rows), rows)]
    own_from = pl.ds(pl.multiple_of(tp_rank * part, part), part)
    peer_from = pl.ds(pl.multiple_of((1 - tp_rank) * part, part), part)
    tile = width // 4
    tiles = [slice(index * tile, (index + 1) * tile) for index in range(4)]
    for columns in tiles:
        mixed[:, columns] = jnp.dot(
            own_part, output_weight[own_from, columns], preferred_element_type=jnp.float32
        )
    trade.wait()
    for columns in tiles:
        mixed[:, columns] += jnp.dot(
            swapped[...], output_weight[peer_from, columns], preferred_element_type=jnp.float32
        )
    mixer_gain = mixer_gain_ref[...].astype(jnp.float32).reshape(1, -1)
    routed_gain = routed_gain_ref[...].astype(jnp.float32).reshape(1, -1)
    final_gain = final_gain_ref[...].astype(jnp.float32).reshape(1, -1)
    chunk = 32

    def normalise(index, carry):
        here = pl.ds(pl.multiple_of(index * chunk, chunk), chunk)
        value = (
            residual[here].astype(jnp.float32) + scaled(mixed[here], mixer_gain)
        ).astype(jnp.bfloat16)
        stream[here] = value
        wide[here] = scaled(value.astype(jnp.float32), routed_gain).astype(jnp.bfloat16)
        return carry

    lax.fori_loop(0, rows // chunk, normalise, 0)
    for columns in tiles:
        send_ref[:, columns] = jnp.dot(
            placing, wide[:, columns], preferred_element_type=jnp.float32
        ).astype(jnp.bfloat16)

    def dispatch(step):
        phase = step // per
        spot = lax.rem(step + place, per)
        dest = other_plane(plane, phase) * per + spot
        return dest, pltpu.make_async_remote_copy(
            send_ref.at[block(dest)],
            arrived.at[phase, block(place)],
            send_sem.at[step],
            recv_sem.at[phase * per + place],
            device_id={"sp": dest},
        )

    own_in = pltpu.make_async_copy(
        send_ref.at[block(me)],
        arrived.at[PHASES - 1, block(place)],
        recv_sem.at[(PHASES - 1) * per + place],
    )

    def start_dispatch(step, carry):
        dest, copy = dispatch(step)

        @pl.when(dest != me)
        def _():
            copy.start()

        return carry

    lax.fori_loop(0, count, start_dispatch, 0)
    own_in.start()

    def end_share(step, carry):
        settle(
            arrived_share.at[step // per, block(lax.rem(step, per))], spread_recv.at[step]
        )
        return carry

    lax.fori_loop(0, count, end_share, 0)
    share_forward = pltpu.make_async_remote_copy(
        arrived_share.at[:, pl.ds(0, half)],
        arrived_share.at[:, pl.ds(half, half)],
        swap_sem.at[2],
        swap_sem.at[3],
        device_id={"tp": 1 - tp_rank},
    )
    share_forward.start()
    for load in loads:
        load.wait()
    share_forward.wait()

    def back(step):
        phase = step // per
        spot = lax.rem(step + place, per)
        dest = other_plane(plane, phase) * per + spot
        return dest, spot, pltpu.make_async_remote_copy(
            result.at[phase, block(spot)],
            fetched.at[block(me)],
            back_send.at[step],
            back_recv.at[me],
            device_id={"sp": dest},
        )

    own_back = pltpu.make_async_copy(
        result.at[PHASES - 1, block(place)], fetched.at[block(me)], back_recv.at[me]
    )

    def serve(phase, carry):
        def land(spot, inner):
            settle(arrived.at[phase, block(spot)], recv_sem.at[phase * per + spot])
            return inner

        lax.fori_loop(0, per, land, 0)
        forward = pltpu.make_async_remote_copy(
            arrived.at[phase, pl.ds(0, half)],
            arrived.at[phase, pl.ds(half, half)],
            forward_send.at[phase],
            forward_recv.at[phase],
            device_id={"tp": 1 - tp_rank},
        )
        forward.start()
        forward.wait()
        share = arrived_share[phase].astype(jnp.float32)
        for expert in range(experts):
            given = arrived[phase]
            gate = jnp.dot(given, gates[expert], preferred_element_type=jnp.float32)
            upper = jnp.dot(given, ups[expert], preferred_element_type=jnp.float32)
            silu = gate / (1.0 + jnp.exp(-gate))
            weighted = silu * upper * share[:, expert : expert + 1]
            hidden[:, expert * units : (expert + 1) * units] = weighted.astype(jnp.bfloat16)
        for columns in tiles:
            product = jnp.dot(hidden[...], downs[:, columns], preferred_element_type=jnp.float32)
            kept[:, columns] = product[:half]
            outgoing[phase, :, columns] = product[half:].astype(jnp.bfloat16)
        swap = pltpu.make_async_remote_copy(
            outgoing.at[phase],
            incoming.at[phase],
            part_send.at[phase],
            part_recv.at[phase],
            device_id={"tp": 1 - tp_rank},
        )
        swap.start()
        swap.wait()
        result[phase] = (kept[...] + incoming[phase].astype(jnp.float32)).astype(jnp.bfloat16)

        def start_back(spot, inner):
            dest, _, copy = back(phase * per + spot)

            @pl.when(dest != me)
            def _():
                copy.start()

            return inner

        lax.fori_loop(0, per, start_back, 0)
        return carry

    lax.fori_loop(0, PHASES, serve, 0)
    own_back.start()

    def finish(step, carry):
        settle(fetched.at[block(step)], back_recv.at[step])
        dest, copy = dispatch(step)
        _, _, home = back(step)
        _, spread_out = share_copy(step)

        @pl.when(dest != me)
        def _():
            copy.wait_send()
            home.wait_send()
            spread_out.wait_send()

        return carry

    lax.fori_loop(0, count, finish, 0)
    for columns in tiles:
        mixed[:, columns] = jnp.dot(
            pick[...], fetched[:, columns], preferred_element_type=jnp.float32
        )

    def update(index, carry):
        here = pl.ds(pl.multiple_of(index * chunk, chunk), chunk)
        out_ref[here] = (
            stream[here].astype(jnp.float32) + scaled(mixed[here], final_gain)
        ).astype(jnp.bfloat16)
        return carry

    lax.fori_loop(0, rows // chunk, update, 0)


def local(
    pool_input,
    documents,
    residual,
    group_weights,
    pool_gain,
    output_weight,
    mixer_gain,
    routed_gain,
    final_gain,
    chosen_group,
    chosen_experts,
    expert_share,
    expert_gate,
    expert_up,
    expert_down,
):
    count = lax.axis_size("sp")
    docs = count // 4
    rows, width = residual.shape
    length, part = pool_input.shape
    reach = length // 2
    cap = length // count
    slots = count * cap
    per = count // PHASES
    half = per * cap
    deep = max(8, docs)
    down = expert_down.reshape(-1, width)
    bf16, f32 = jnp.bfloat16, jnp.float32
    dma, vmem = pltpu.SemaphoreType.DMA, pltpu.VMEM
    whole = pl.BlockSpec(memory_space=pltpu.VMEM)
    outside = pl.BlockSpec(memory_space=pl.ANY)
    return pl.pallas_call(
        functools.partial(layer_kernel, count, docs),
        out_shape=jax.ShapeDtypeStruct((rows, width), bf16),
        in_specs=[whole, whole, outside, whole, whole, outside]
        + [whole] * 6
        + [outside] * 3,
        out_specs=whole,
        scratch_shapes=[
            vmem((length + 2 * reach, part), bf16),
            vmem((2, 1, reach), documents.dtype),
            vmem((deep, part + LANES), f32),
            vmem((count, deep, part + LANES), f32),
            vmem((length, part), bf16),
            vmem((rows, part), bf16),
            vmem(output_weight.shape, bf16),
            vmem((rows, width), bf16),
            vmem((rows, width), f32),
            vmem((rows, width), bf16),
            vmem((rows, width), bf16),
            vmem((rows, slots), bf16),
            vmem((slots, LANES), bf16),
            vmem((PHASES, 2 * half, LANES), bf16),
            vmem((slots, width), bf16),
            vmem((slots, width), bf16),
            vmem((PHASES, 2 * half, width), bf16),
            vmem(expert_gate.shape, bf16),
            vmem(expert_up.shape, bf16),
            vmem(down.shape, bf16),
            vmem((2 * half, down.shape[0]), bf16),
            vmem((half, width), f32),
            vmem((PHASES, half, width), bf16),
            vmem((PHASES, half, width), bf16),
            vmem((PHASES, half, width), bf16),
            dma((4,)),
            dma((5,)),
            dma((count,)),
            dma((count,)),
            dma((4,)),
            dma((count,)),
            dma((count,)),
            dma((5,)),
            dma((count,)),
            dma((count,)),
            dma((PHASES,)),
            dma((PHASES,)),
            dma((PHASES,)),
            dma((PHASES,)),
            dma((count,)),
            dma((count,)),
        ],
        compiler_params=pltpu.CompilerParams(
            collective_id=0, has_side_effects=True, vmem_limit_bytes=60 * 1024 * 1024
        ),
    )(
        pool_input,
        documents.reshape(2, 1, reach),
        residual,
        group_weights,
        pool_gain,
        output_weight,
        mixer_gain,
        routed_gain,
        final_gain,
        chosen_group.T,
        chosen_experts.T,
        expert_share.T,
        expert_gate,
        expert_up,
        down,
    )


def solution(mesh):
    placed = (
        P("sp", "tp"),
        P("sp"),
        P(("sp", "tp"), None),
        P(),
        P(),
        P(),
        P(),
        P(),
        P(),
        P(("sp", "tp"), None),
        P(("sp", "tp"), None),
        P(("sp", "tp"), None),
        P("sp", None, "tp"),
        P("sp", None, "tp"),
        P("sp", "tp", None),
    )
    return jax.shard_map(
        local, mesh=mesh, in_specs=placed, out_specs=P(("sp", "tp"), None), check_vma=False
    )
```

profile of v0, /device:TPU:0, one launch (start us, length us, event | category | flops | bytes accessed | tf_op | source)
XLA Modules:
  0.0 129.9 jit_solution(4313516934124602602)
XLA Ops:
  0.0 127.6 %shard_map.145 = bf16[256,2048]{1,0:T(8,128)(2,1)} custom-call(bf16[512,256]{1,0:T(8,128)(2,1)} %pool_ref.1, s32[2,1,256]{2,1,0:T(1,128)} %bitcast.6, bf16[256,2048]{1,0:T(8,128)(2,1)} %residual_hbm.1, bf16[8,64,64]{2,1,0:T(8,128)(2,1)} %weights_ref.1, bf16[512]{0:T(512)(128)(2,1)} %pool_gain_ref.1, bf16[512,2048]{1,0:T(8,128)(2,1)} %output_hbm.1, ...), custom_call_target="tpu_custom_call" | custom-call | tf_op jit(solution)/shard_map/pallas_call | solution.py:587
  127.6 2.3 %copy.17 = bf16[256,2048]{1,0:T(8,128)(2,1)} copy(bf16[256,2048]{1,0:T(8,128)(2,1)} %shard_map.145) | data formatting | bytes 2097152
where the time goes:
time: 130 us
  Pallas kernels  128 us (98%)
  local copies, waits for them, and re-layouts  2.3 us (2%)
    pallas_call x1, Pallas kernels, local(): pl.pallas_call(functools.partial(layer_kernel, count, docs), out_shape=ja...  128 us

commit v1 on v0

--- a/solution.py
+++ b/solution.py
@@ -11,6 +11,9 @@
 
 
 PHASES = 4
+EARLY = 2
+SEND_ORDER = (3, 0, 2, 1)
+SERVE_ORDER = (3, 0, 2, 1)
 LANES = 128
 
 
@@ -25,6 +28,13 @@
 
     lax.fori_loop(1, count, signal, 0)
     pl.semaphore_signal(barrier, inc=1, device_id={"tp": 1 - lax.axis_index("tp")})
+
+
+def in_order(turn, order):
+    phase = order[-1]
+    for index in range(len(order) - 2, -1, -1):
+        phase = jnp.where(turn == index, order[index], phase)
+    return phase
 
 
 def settle(ref, sem):
@@ -61,38 +71,43 @@
     length, part = pool_ref.shape
     reach = length // 2
     barrier = pltpu.get_barrier_semaphore()
-    own_rows = pltpu.make_async_copy(pool_ref, padded.at[pl.ds(reach, length)], edge_recv.at[4])
+    own_rows = pltpu.make_async_copy(pool_ref, padded.at[pl.ds(reach, length)], edge_recv.at[6])
     own_rows.start()
     own_docs = jnp.concatenate([docs_ref[0], docs_ref[1]], axis=1).astype(jnp.float32)
-    deep = table.shape[0]
+    group_dim = weights_ref.shape[1]
+    low, high = slice(0, LANES), slice(part - LANES, part)
     hot = (
-        lax.broadcasted_iota(jnp.int32, (deep, length), 0).astype(jnp.float32) == own_docs
+        lax.broadcasted_iota(jnp.int32, (docs, length), 0).astype(jnp.float32) == own_docs
     ).astype(jnp.float32)
-    table[:, :part] = jnp.dot(
-        hot.astype(jnp.bfloat16), pool_ref[...], preferred_element_type=jnp.float32
-    )
-    table[:, part:] = jnp.broadcast_to(jnp.sum(hot, axis=1, keepdims=True), (deep, LANES))
+    sums = jnp.dot(
+        hot.astype(jnp.bfloat16), pool_ref[:, high], preferred_element_type=jnp.float32
+    )
+    global_lane = lax.broadcasted_iota(jnp.int32, (docs, LANES), 1) >= LANES - group_dim
+    table[...] = jnp.where(global_lane, sums, jnp.sum(hot, axis=1, keepdims=True))
     local_copy = pltpu.make_async_copy(table, tables.at[me], table_recv.at[me])
     local_copy.start()
     pl.semaphore_wait(barrier, count)
     right, left = lax.rem(me + 1, count), lax.rem(me + count - 1, count)
     copies = []
-    for side, (start, target) in enumerate(((reach, right), (0, left))):
-        copies.append(
-            pltpu.make_async_remote_copy(
-                pool_ref.at[pl.ds(start, reach)],
-                padded.at[pl.ds(side * (length + reach), reach)],
-                edge_send.at[side],
-                edge_recv.at[side],
-                device_id={"sp": target},
+    for side, target in enumerate((right, left)):
+        for nth, (columns, deep) in enumerate(((low, reach // 2), (high, reach))):
+            start = (length - deep) if side == 0 else 0
+            into = (reach - deep) if side == 0 else (reach + length)
+            copies.append(
+                pltpu.make_async_remote_copy(
+                    pool_ref.at[pl.ds(start, deep), columns],
+                    padded.at[pl.ds(into, deep), columns],
+                    edge_send.at[3 * side + nth],
+                    edge_recv.at[3 * side + nth],
+                    device_id={"sp": target},
+                )
             )
-        )
         copies.append(
             pltpu.make_async_remote_copy(
                 docs_ref.at[1 - side],
                 edge_docs.at[side],
-                edge_send.at[2 + side],
-                edge_recv.at[2 + side],
+                edge_send.at[3 * side + 2],
+                edge_recv.at[3 * side + 2],
                 device_id={"sp": target},
             )
         )
@@ -117,7 +132,6 @@
     spread()
 
     local_groups = part // weights_ref.shape[1]
-    group_dim = weights_ref.shape[1]
     bands = []
     for group in range(local_groups):
         own = weights_ref[tp_rank * local_groups + group]
@@ -132,13 +146,8 @@
         gain = jnp.where(tp_rank == other, rest, gain)
     own_column = jnp.transpose(jnp.broadcast_to(own_docs, (LANES, length)))[:, :1]
     block = length // 4
-    span = block + 2 * reach
-    offsets = (
-        lax.broadcasted_iota(jnp.int32, (block, span), 1)
-        - reach
-        - lax.broadcasted_iota(jnp.int32, (block, span), 0)
-    )
-    levels = lax.rem(lax.broadcasted_iota(jnp.int32, (block, part), 1) // group_dim, 4)
+    lane_group = lax.broadcasted_iota(jnp.int32, (block, LANES), 1) // group_dim
+    first_half = lane_group == 0
     own_rows.wait()
     for copy in copies:
         copy.wait()
@@ -152,25 +161,44 @@
 
     lax.fori_loop(0, count, end_table, 0)
     totals = jnp.sum(tables[...], axis=0)
-    doc_means = totals[:, :part] / totals[:, part : part + 1]
+    doc_means = totals / totals[:, :1]
     for index in range(length // block):
         rows = slice(index * block, (index + 1) * block)
-        reached = slice(index * block, index * block + span)
         column = own_column[rows]
-        same = all_docs[:, reached] == column
-        values = padded[reached]
-        mean = jnp.zeros((block, part), jnp.float32)
-        for doc in range(docs):
-            mean = jnp.where(column == doc, doc_means[doc : doc + 1], mean)
-        for level in range(3):
+
+        def window_mean(level, columns):
             half_width = length * (1 << level) // 8
-            inside = same & (offsets >= -half_width) & (offsets < half_width)
+            span = block + 2 * half_width
+            start = reach + index * block - half_width
+            offsets = (
+                lax.broadcasted_iota(jnp.int32, (block, span), 1)
+                - half_width
+                - lax.broadcasted_iota(jnp.int32, (block, span), 0)
+            )
+            reached = slice(start, start + span)
+            inside = (
+                (all_docs[:, reached] == column)
+                & (offsets >= -half_width)
+                & (offsets < half_width)
+            )
             mask = jnp.where(inside, 1.0, 0.0)
             sums = jnp.dot(
-                mask.astype(jnp.bfloat16), values, preferred_element_type=jnp.float32
+                mask.astype(jnp.bfloat16),
+                padded[reached, columns],
+                preferred_element_type=jnp.float32,
             )
-            sizes = jnp.sum(mask, axis=1, keepdims=True)
-            mean = jnp.where(levels == level, sums / sizes, mean)
+            return sums / jnp.sum(mask, axis=1, keepdims=True)
+
+        doc_mean = jnp.zeros((block, LANES), jnp.float32)
+        for doc in range(docs):
+            doc_mean = jnp.where(column == doc, doc_means[doc : doc + 1], doc_mean)
+        mean = jnp.concatenate(
+            [
+                jnp.where(first_half, window_mean(0, low), window_mean(1, low)),
+                jnp.where(first_half, window_mean(2, high), doc_mean),
+            ],
+            axis=1,
+        )
         difference = (mean - pool_ref[rows].astype(jnp.float32)).astype(jnp.bfloat16)
         pooled[rows] = (
             jnp.dot(difference, block_weight, preferred_element_type=jnp.float32) * gain
@@ -183,7 +211,7 @@
     lax.fori_loop(1, count, sent_table, 0)
 
 
-def route(group_ref, experts_ref, share_ref, cap, slots, pick, share_send):
+def route(group_ref, experts_ref, share_ref, cap, slots, place, pick, share_send):
     rows = group_ref.shape[1]
     ids = group_ref[...]
     names = lax.broadcasted_iota(jnp.int32, (LANES, rows), 0)
@@ -203,16 +231,22 @@
         slot == lax.broadcasted_iota(jnp.int32, (slots, rows), 0).astype(jnp.float32)
     ).astype(jnp.float32)
     pick[...] = jnp.transpose(chosen).astype(jnp.bfloat16)
-    placing = chosen.astype(jnp.bfloat16)
+    place[...] = chosen.astype(jnp.bfloat16)
+    spot = lax.broadcasted_iota(jnp.int32, (LANES, rows), 0)
+    named = spot // cap
     total = jnp.zeros((LANES, rows), jnp.float32)
     for nth in range(experts_ref.shape[0]):
-        named = experts_ref[nth : nth + 1] == names
-        total = total + jnp.where(named, share_ref[nth : nth + 1].astype(jnp.float32), 0.0)
-    shares = jnp.transpose(total).astype(jnp.bfloat16)
-    share_send[...] = jnp.dot(placing, shares, preferred_element_type=jnp.float32).astype(
-        jnp.bfloat16
-    )
-    return placing
+        here = experts_ref[nth : nth + 1] == named
+        total = total + jnp.where(here, share_ref[nth : nth + 1].astype(jnp.float32), 0.0)
+    total = jnp.where(rank == lax.rem(spot, cap).astype(jnp.float32), total, 0.0)
+    sent = lax.dot_general(
+        member.astype(jnp.bfloat16),
+        total.astype(jnp.bfloat16),
+        (((1,), (1,)), ((), ())),
+        preferred_element_type=jnp.float32,
+    )
+    for dest in range(slots // cap):
+        share_send[dest] = sent[dest : dest + 1]
 
 
 def scaled(values, gain):
@@ -249,9 +283,15 @@
     mixed,
     stream,
     wide,
+    place,
     pick,
     share_send,
     arrived_share,
+    early_send,
+    early_recv,
+    pooled_send,
+    pooled_recv,
+    far_mixed,
     send_ref,
     fetched,
     arrived,
@@ -279,10 +319,14 @@
     part_recv,
     back_send,
     back_recv,
+    first_send,
+    first_recv,
+    second_send,
+    second_recv,
 ):
     me, tp_rank = lax.axis_index("sp"), lax.axis_index("tp")
     per = count // PHASES
-    plane, place = me // per, lax.rem(me, per)
+    plane, spot_of = me // per, lax.rem(me, per)
     rows, width = out_ref.shape
     slots = send_ref.shape[0]
     cap = slots // count
@@ -296,37 +340,65 @@
 
     def target(step):
         phase = step // per
-        spot = lax.rem(step + place, per)
+        spot = lax.rem(step + spot_of, per)
         return phase, spot, other_plane(plane, phase) * per + spot
 
-    early = [
-        pltpu.make_async_copy(output_hbm, output_weight, weight_sem.at[3]),
-        pltpu.make_async_copy(residual_hbm, residual, weight_sem.at[4]),
-    ]
+    residual_load = pltpu.make_async_copy(residual_hbm, residual, weight_sem.at[4])
+    output_load = pltpu.make_async_copy(output_hbm, output_weight, weight_sem.at[3])
     loads = [
         pltpu.make_async_copy(gate_hbm, gates, weight_sem.at[0]),
         pltpu.make_async_copy(up_hbm, ups, weight_sem.at[1]),
         pltpu.make_async_copy(down_hbm, downs, weight_sem.at[2]),
     ]
-    for load in early + loads:
+    for load in [residual_load, output_load] + loads:
         load.start()
-    placing = route(group_ref, experts_ref, share_ref, cap, slots, pick, share_send)
+    route(group_ref, experts_ref, share_ref, cap, slots, place, pick, share_send)
+    tile = width // 4
+    tiles = [slice(index * tile, (index + 1) * tile) for index in range(4)]
+
+    def far_dest(step):
+        return other_plane(plane, 0) * per + lax.rem(step + spot_of, per)
+
+    far_place = jnp.concatenate([place[block(far_dest(step))] for step in range(EARLY)], axis=0)
+    residual_load.wait()
+    for columns in tiles:
+        early_send[:, columns] = jnp.dot(
+            far_place, residual[:, columns], preferred_element_type=jnp.float32
+        ).astype(jnp.bfloat16)
+
+    def far_copies(step):
+        here = pl.ds(step * cap, cap)
+        return [
+            pltpu.make_async_remote_copy(
+                source.at[here],
+                into.at[here],
+                send.at[step],
+                recv.at[step],
+                device_id={"sp": far_dest(step)},
+            )
+            for source, into, send, recv in (
+                (early_send, early_recv, first_send, first_recv),
+                (pooled_send, pooled_recv, second_send, second_recv),
+            )
+        ]
+
+    far = [far_copies(step) for step in range(EARLY)]
 
     def share_copy(step):
         phase, _, dest = target(step)
         return dest, pltpu.make_async_remote_copy(
-            share_send.at[block(dest)],
-            arrived_share.at[phase, block(place)],
+            share_send.at[dest],
+            arrived_share.at[phase, 0, spot_of],
             spread_send.at[step],
-            spread_recv.at[phase * per + place],
+            spread_recv.at[phase * per + spot_of],
             device_id={"sp": dest},
         )
 
     def spread():
         pltpu.make_async_copy(
-            share_send.at[block(me)],
-            arrived_share.at[PHASES - 1, block(place)],
-            spread_recv.at[(PHASES - 1) * per + place],
+            share_send.at[me],
+            arrived_share.at[PHASES - 1, 0, spot_of],
+            spread_recv.at[(PHASES - 1) * per + spot_of],
         ).start()
 
         def start_share(step, carry):
@@ -339,6 +411,8 @@
             return carry
 
         lax.fori_loop(0, count, start_share, 0)
+        for first, _ in far:
+            first.start()
 
     mixer_stage(
         count,
@@ -368,18 +442,23 @@
         device_id={"tp": 1 - tp_rank},
     )
     trade.start()
-    for load in early:
-        load.wait()
+    output_load.wait()
     own_part = pooled[pl.ds(pl.multiple_of(tp_rank * rows, rows), rows)]
     own_from = pl.ds(pl.multiple_of(tp_rank * part, part), part)
     peer_from = pl.ds(pl.multiple_of((1 - tp_rank) * part, part), part)
-    tile = width // 4
-    tiles = [slice(index * tile, (index + 1) * tile) for index in range(4)]
+    pooled_send[:, own_from] = jnp.dot(
+        far_place, own_part, preferred_element_type=jnp.float32
+    ).astype(jnp.bfloat16)
     for columns in tiles:
         mixed[:, columns] = jnp.dot(
             own_part, output_weight[own_from, columns], preferred_element_type=jnp.float32
         )
     trade.wait()
+    pooled_send[:, peer_from] = jnp.dot(
+        far_place, swapped[...], preferred_element_type=jnp.float32
+    ).astype(jnp.bfloat16)
+    for _, second in far:
+        second.start()
     for columns in tiles:
         mixed[:, columns] += jnp.dot(
             swapped[...], output_weight[peer_from, columns], preferred_element_type=jnp.float32
@@ -399,27 +478,22 @@
         return carry
 
     lax.fori_loop(0, rows // chunk, normalise, 0)
-    for columns in tiles:
-        send_ref[:, columns] = jnp.dot(
-            placing, wide[:, columns], preferred_element_type=jnp.float32
-        ).astype(jnp.bfloat16)
-
     def dispatch(step):
         phase = step // per
-        spot = lax.rem(step + place, per)
+        spot = lax.rem(step + spot_of, per)
         dest = other_plane(plane, phase) * per + spot
         return dest, pltpu.make_async_remote_copy(
             send_ref.at[block(dest)],
-            arrived.at[phase, block(place)],
+            arrived.at[phase, block(spot_of)],
             send_sem.at[step],
-            recv_sem.at[phase * per + place],
+            recv_sem.at[phase * per + spot_of],
             device_id={"sp": dest},
         )
 
     own_in = pltpu.make_async_copy(
         send_ref.at[block(me)],
-        arrived.at[PHASES - 1, block(place)],
-        recv_sem.at[(PHASES - 1) * per + place],
+        arrived.at[PHASES - 1, block(spot_of)],
+        recv_sem.at[(PHASES - 1) * per + spot_of],
     )
 
     def start_dispatch(step, carry):
@@ -431,19 +505,27 @@
 
         return carry
 
-    lax.fori_loop(0, count, start_dispatch, 0)
-    own_in.start()
+    for phase in SEND_ORDER:
+        there = pl.ds(pl.multiple_of(other_plane(plane, phase) * half, half), half)
+        for columns in tiles:
+            send_ref[there, columns] = jnp.dot(
+                place[there], wide[:, columns], preferred_element_type=jnp.float32
+            ).astype(jnp.bfloat16)
+        begin = EARLY if phase == 0 else phase * per
+        lax.fori_loop(begin, (phase + 1) * per, start_dispatch, 0)
+        if phase == PHASES - 1:
+            own_in.start()
 
     def end_share(step, carry):
         settle(
-            arrived_share.at[step // per, block(lax.rem(step, per))], spread_recv.at[step]
+            arrived_share.at[step // per, 0, lax.rem(step, per)], spread_recv.at[step]
         )
         return carry
 
     lax.fori_loop(0, count, end_share, 0)
     share_forward = pltpu.make_async_remote_copy(
-        arrived_share.at[:, pl.ds(0, half)],
-        arrived_share.at[:, pl.ds(half, half)],
+        arrived_share.at[:, 0],
+        arrived_share.at[:, 1],
         swap_sem.at[2],
         swap_sem.at[3],
         device_id={"tp": 1 - tp_rank},
@@ -455,7 +537,7 @@
 
     def back(step):
         phase = step // per
-        spot = lax.rem(step + place, per)
+        spot = lax.rem(step + spot_of, per)
         dest = other_plane(plane, phase) * per + spot
         return dest, spot, pltpu.make_async_remote_copy(
             result.at[phase, block(spot)],
@@ -466,15 +548,59 @@
         )
 
     own_back = pltpu.make_async_copy(
-        result.at[PHASES - 1, block(place)], fetched.at[block(me)], back_recv.at[me]
-    )
-
-    def serve(phase, carry):
-        def land(spot, inner):
+        result.at[PHASES - 1, block(spot_of)], fetched.at[block(me)], back_recv.at[me]
+    )
+
+    def meet_far():
+        for step in range(EARLY):
+            for copy in far[step]:
+                copy.wait_recv()
+        for columns in tiles:
+            far_mixed[:, columns] = jnp.dot(
+                pooled_recv[...], output_weight[:, columns], preferred_element_type=jnp.float32
+            )
+        for step in range(EARLY):
+            here = pl.ds(step * cap, cap)
+            value = (
+                early_recv[here].astype(jnp.float32) + scaled(far_mixed[here], mixer_gain)
+            ).astype(jnp.bfloat16)
+            arrived[0, block(lax.rem(spot_of + per - step, per))] = scaled(
+                value.astype(jnp.float32), routed_gain
+            ).astype(jnp.bfloat16)
+
+    def start_back(step, carry):
+        dest, _, copy = back(step)
+
+        @pl.when(dest != me)
+        def _():
+            copy.start()
+
+        return carry
+
+    def return_phase(phase):
+        lax.fori_loop(phase * per, (phase + 1) * per, start_back, 0)
+
+    def sent_near(step, carry):
+        dispatch(step)[1].wait_send()
+        return carry
+
+    def serve(turn, carry):
+        phase = in_order(turn, SERVE_ORDER)
+        pieces = [arrived_share[phase, core, spot] for core in range(2) for spot in range(per)]
+        pieces.append(jnp.zeros((LANES - 2 * per, LANES), jnp.float32))
+        turned = jnp.transpose(jnp.concatenate(pieces, axis=0))
+
+        def land(step, inner):
+            spot = lax.rem(spot_of + per - step, per)
             settle(arrived.at[phase, block(spot)], recv_sem.at[phase * per + spot])
             return inner
 
-        lax.fori_loop(0, per, land, 0)
+        lax.fori_loop(jnp.where(phase == 0, EARLY, 0), per, land, 0)
+
+        @pl.when(phase == 0)
+        def _():
+            meet_far()
+
         forward = pltpu.make_async_remote_copy(
             arrived.at[phase, pl.ds(0, half)],
             arrived.at[phase, pl.ds(half, half)],
@@ -484,13 +610,16 @@
         )
         forward.start()
         forward.wait()
-        share = arrived_share[phase].astype(jnp.float32)
         for expert in range(experts):
             given = arrived[phase]
             gate = jnp.dot(given, gates[expert], preferred_element_type=jnp.float32)
             upper = jnp.dot(given, ups[expert], preferred_element_type=jnp.float32)
             silu = gate / (1.0 + jnp.exp(-gate))
-            weighted = silu * upper * share[:, expert : expert + 1]
+            span = slice(expert * cap, (expert + 1) * cap)
+            share = jnp.concatenate(
+                [turned[span, column : column + 1] for column in range(2 * per)], axis=0
+            )
+            weighted = silu * upper * share
             hidden[:, expert * units : (expert + 1) * units] = weighted.astype(jnp.bfloat16)
         for columns in tiles:
             product = jnp.dot(hidden[...], downs[:, columns], preferred_element_type=jnp.float32)
@@ -507,16 +636,20 @@
         swap.wait()
         result[phase] = (kept[...] + incoming[phase].astype(jnp.float32)).astype(jnp.bfloat16)
 
-        def start_back(spot, inner):
-            dest, _, copy = back(phase * per + spot)
-
-            @pl.when(dest != me)
-            def _():
-                copy.start()
-
-            return inner
-
-        lax.fori_loop(0, per, start_back, 0)
+        @pl.when(phase == 3)
+        def _():
+            return_phase(3)
+
+        @pl.when(phase == 2)
+        def _():
+            lax.fori_loop(per, 2 * per, sent_near, 0)
+            return_phase(0)
+            return_phase(2)
+
+        @pl.when(phase == 1)
+        def _():
+            return_phase(1)
+
         return carry
 
     lax.fori_loop(0, PHASES, serve, 0)
@@ -528,14 +661,20 @@
         _, _, home = back(step)
         _, spread_out = share_copy(step)
 
+        @pl.when((dest != me) & (step >= EARLY) & (step // per != 1))
+        def _():
+            copy.wait_send()
+
         @pl.when(dest != me)
         def _():
-            copy.wait_send()
             home.wait_send()
             spread_out.wait_send()
 
         return carry
 
+    for first, second in far:
+        first.wait_send()
+        second.wait_send()
     lax.fori_loop(0, count, finish, 0)
     for columns in tiles:
         mixed[:, columns] = jnp.dot(
@@ -578,7 +717,6 @@
     slots = count * cap
     per = count // PHASES
     half = per * cap
-    deep = max(8, docs)
     down = expert_down.reshape(-1, width)
     bf16, f32 = jnp.bfloat16, jnp.float32
     dma, vmem = pltpu.SemaphoreType.DMA, pltpu.VMEM
@@ -594,8 +732,8 @@
         scratch_shapes=[
             vmem((length + 2 * reach, part), bf16),
             vmem((2, 1, reach), documents.dtype),
-            vmem((deep, part + LANES), f32),
-            vmem((count, deep, part + LANES), f32),
+            vmem((docs, LANES), f32),
+            vmem((count, docs, LANES), f32),
             vmem((length, part), bf16),
             vmem((rows, part), bf16),
             vmem(output_weight.shape, bf16),
@@ -603,9 +741,15 @@
             vmem((rows, width), f32),
             vmem((rows, width), bf16),
             vmem((rows, width), bf16),
+            vmem((slots, rows), bf16),
             vmem((rows, slots), bf16),
-            vmem((slots, LANES), bf16),
-            vmem((PHASES, 2 * half, LANES), bf16),
+            vmem((count, 1, LANES), f32),
+            vmem((PHASES, 2, per, 1, LANES), f32),
+            vmem((EARLY * cap, width), bf16),
+            vmem((EARLY * cap, width), bf16),
+            vmem((EARLY * cap, 2 * part), bf16),
+            vmem((EARLY * cap, 2 * part), bf16),
+            vmem((EARLY * cap, width), f32),
             vmem((slots, width), bf16),
             vmem((slots, width), bf16),
             vmem((PHASES, 2 * half, width), bf16),
@@ -617,8 +761,8 @@
             vmem((PHASES, half, width), bf16),
             vmem((PHASES, half, width), bf16),
             vmem((PHASES, half, width), bf16),
-            dma((4,)),
-            dma((5,)),
+            dma((6,)),
+            dma((7,)),
             dma((count,)),
             dma((count,)),
             dma((4,)),
@@ -633,6 +777,10 @@
             dma((PHASES,)),
             dma((count,)),
             dma((count,)),
+            dma((EARLY,)),
+            dma((EARLY,)),
+            dma((EARLY,)),
+            dma((EARLY,)),
         ],
         compiler_params=pltpu.CompilerParams(
             collective_id=0, has_side_effects=True, vmem_limit_bytes=60 * 1024 * 1024

time: 130 us -> 116 us (0.89)
  Pallas kernels: 128 us -> 114 us
    pallas_call x1, Pallas kernels: 128 us -> 114 us  [local(): pl.pallas_call(functools.partial(layer_kernel, count, docs), out_shape=ja...]
where the time goes in v1:
time: 116 us
  Pallas kernels  114 us (98%)
  local copies, waits for them, and re-layouts  2.3 us (2%)
    pallas_call x1, Pallas kernels, local(): pl.pallas_call(functools.partial(layer_kernel, count, docs), out_shape=ja...  114 us

profile of v1, /device:TPU:0, one launch (start us, length us, event | category | flops | bytes accessed | tf_op | source)
XLA Modules:
  0.0 116.3 jit_solution(16200170118593443292)
XLA Ops:
  0.0 114.0 %shard_map.145 = bf16[256,2048]{1,0:T(8,128)(2,1)} custom-call(bf16[512,256]{1,0:T(8,128)(2,1)} %pool_ref.1, s32[2,1,256]{2,1,0:T(1,128)} %bitcast.6, bf16[256,2048]{1,0:T(8,128)(2,1)} %residual_hbm.1, bf16[8,64,64]{2,1,0:T(8,128)(2,1)} %weights_ref.1, bf16[512]{0:T(512)(128)(2,1)} %pool_gain_ref.1, bf16[512,2048]{1,0:T(8,128)(2,1)} %output_hbm.1, ...), custom_call_target="tpu_custom_call" | custom-call | tf_op jit(solution)/shard_map/pallas_call | solution.py:725
  114.0 2.3 %copy.17 = bf16[256,2048]{1,0:T(8,128)(2,1)} copy(bf16[256,2048]{1,0:T(8,128)(2,1)} %shard_map.145) | data formatting | bytes 2097152

commit v2 on v1

--- a/solution.py
+++ b/solution.py
@@ -11,7 +11,10 @@
 
 
 PHASES = 4
-EARLY = 2
+EARLY = 3
+EAGER = 1
+HOLDTURN = 1
+FINISH_ORDER = (3, 2, 0, 1)
 SEND_ORDER = (3, 0, 2, 1)
 SERVE_ORDER = (3, 0, 2, 1)
 LANES = 128
@@ -58,6 +61,8 @@
     weights_ref,
     pool_gain_ref,
     padded,
+    packed,
+    unpacked,
     edge_docs,
     table,
     tables,
@@ -84,40 +89,48 @@
     )
     global_lane = lax.broadcasted_iota(jnp.int32, (docs, LANES), 1) >= LANES - group_dim
     table[...] = jnp.where(global_lane, sums, jnp.sum(hot, axis=1, keepdims=True))
-    local_copy = pltpu.make_async_copy(table, tables.at[me], table_recv.at[me])
+    deep = reach // 2
+    front = lax.broadcasted_iota(jnp.int32, (deep, LANES), 1) < group_dim
+    for side, start in enumerate((length - reach, 0)):
+        first = pool_ref[pl.ds(start, deep), high].astype(jnp.float32)
+        second = pool_ref[pl.ds(start + deep, deep), high].astype(jnp.float32)
+        packed[side] = jnp.where(
+            front, first, pltpu.roll(second, group_dim, 1)
+        ).astype(jnp.bfloat16)
+    local_copy = pltpu.make_async_copy(table, tables.at[me], table_recv.at[0])
     local_copy.start()
     pl.semaphore_wait(barrier, count)
     right, left = lax.rem(me + 1, count), lax.rem(me + count - 1, count)
     copies = []
     for side, target in enumerate((right, left)):
-        for nth, (columns, deep) in enumerate(((low, reach // 2), (high, reach))):
-            start = (length - deep) if side == 0 else 0
-            into = (reach - deep) if side == 0 else (reach + length)
+        start = length - deep if side == 0 else 0
+        into = reach - deep if side == 0 else reach + length
+        for nth, (source, place) in enumerate(
+            (
+                (
+                    pool_ref.at[pl.ds(start, deep), low],
+                    padded.at[pl.ds(into, deep), low],
+                ),
+                (packed.at[side], unpacked.at[side]),
+                (docs_ref.at[1 - side], edge_docs.at[side]),
+            )
+        ):
             copies.append(
                 pltpu.make_async_remote_copy(
-                    pool_ref.at[pl.ds(start, deep), columns],
-                    padded.at[pl.ds(into, deep), columns],
+                    source,
+                    place,
                     edge_send.at[3 * side + nth],
                     edge_recv.at[3 * side + nth],
                     device_id={"sp": target},
                 )
             )
-        copies.append(
-            pltpu.make_async_remote_copy(
-                docs_ref.at[1 - side],
-                edge_docs.at[side],
-                edge_send.at[3 * side + 2],
-                edge_recv.at[3 * side + 2],
-                device_id={"sp": target},
-            )
-        )
 
     def table_copy(step):
         return pltpu.make_async_remote_copy(
             table,
             tables.at[me],
-            table_send.at[step],
-            table_recv.at[me],
+            table_send.at[0],
+            table_recv.at[0],
             device_id={"sp": lax.rem(me + step, count)},
         )
 
@@ -151,15 +164,17 @@
     own_rows.wait()
     for copy in copies:
         copy.wait()
+    for side, start in enumerate((0, reach + length)):
+        both = unpacked[side]
+        padded[pl.ds(start, deep), high] = both
+        padded[pl.ds(start + deep, deep), high] = pltpu.roll(
+            both.astype(jnp.float32), LANES - group_dim, 1
+        ).astype(jnp.bfloat16)
     before = jnp.where(me == 0, -1.0, edge_docs[0].astype(jnp.float32))
     after = jnp.where(me == count - 1, -1.0, edge_docs[1].astype(jnp.float32))
     all_docs = jnp.concatenate([before, own_docs, after], axis=1)
 
-    def end_table(step, carry):
-        settle(tables.at[step], table_recv.at[step])
-        return carry
-
-    lax.fori_loop(0, count, end_table, 0)
+    settle(tables, table_recv.at[0])
     totals = jnp.sum(tables[...], axis=0)
     doc_means = totals / totals[:, :1]
     for index in range(length // block):
@@ -204,11 +219,7 @@
             jnp.dot(difference, block_weight, preferred_element_type=jnp.float32) * gain
         ).astype(jnp.bfloat16)
 
-    def sent_table(step, carry):
-        table_copy(step).wait_send()
-        return carry
-
-    lax.fori_loop(1, count, sent_table, 0)
+    settle(tables.at[pl.ds(0, count - 1)], table_send.at[0])
 
 
 def route(group_ref, experts_ref, share_ref, cap, slots, place, pick, share_send):
@@ -271,8 +282,10 @@
     gate_hbm,
     up_hbm,
     down_hbm,
-    out_ref,
+    out_hbm,
     padded,
+    packed,
+    unpacked,
     edge_docs,
     table,
     tables,
@@ -303,6 +316,8 @@
     outgoing,
     incoming,
     result,
+    slot_stream,
+    final,
     edge_send,
     edge_recv,
     table_send,
@@ -323,11 +338,12 @@
     first_recv,
     second_send,
     second_recv,
+    write_sem,
 ):
     me, tp_rank = lax.axis_index("sp"), lax.axis_index("tp")
     per = count // PHASES
     plane, spot_of = me // per, lax.rem(me, per)
-    rows, width = out_ref.shape
+    rows, width = out_hbm.shape
     slots = send_ref.shape[0]
     cap = slots // count
     experts, _, units = gates.shape
@@ -372,8 +388,8 @@
             pltpu.make_async_remote_copy(
                 source.at[here],
                 into.at[here],
-                send.at[step],
-                recv.at[step],
+                send.at[0],
+                recv.at[0],
                 device_id={"sp": far_dest(step)},
             )
             for source, into, send, recv in (
@@ -389,8 +405,8 @@
         return dest, pltpu.make_async_remote_copy(
             share_send.at[dest],
             arrived_share.at[phase, 0, spot_of],
-            spread_send.at[step],
-            spread_recv.at[phase * per + spot_of],
+            spread_send.at[0],
+            spread_recv.at[0],
             device_id={"sp": dest},
         )
 
@@ -398,7 +414,7 @@
         pltpu.make_async_copy(
             share_send.at[me],
             arrived_share.at[PHASES - 1, 0, spot_of],
-            spread_recv.at[(PHASES - 1) * per + spot_of],
+            spread_recv.at[0],
         ).start()
 
         def start_share(step, carry):
@@ -424,6 +440,8 @@
         weights_ref,
         pool_gain_ref,
         padded,
+        packed,
+        unpacked,
         edge_docs,
         table,
         tables,
@@ -485,15 +503,15 @@
         return dest, pltpu.make_async_remote_copy(
             send_ref.at[block(dest)],
             arrived.at[phase, block(spot_of)],
-            send_sem.at[step],
-            recv_sem.at[phase * per + spot_of],
+            send_sem.at[phase],
+            recv_sem.at[phase],
             device_id={"sp": dest},
         )
 
     own_in = pltpu.make_async_copy(
         send_ref.at[block(me)],
         arrived.at[PHASES - 1, block(spot_of)],
-        recv_sem.at[(PHASES - 1) * per + spot_of],
+        recv_sem.at[PHASES - 1],
     )
 
     def start_dispatch(step, carry):
@@ -516,13 +534,14 @@
         if phase == PHASES - 1:
             own_in.start()
 
-    def end_share(step, carry):
-        settle(
-            arrived_share.at[step // per, 0, lax.rem(step, per)], spread_recv.at[step]
-        )
-        return carry
-
-    lax.fori_loop(0, count, end_share, 0)
+    for phase in range(PHASES):
+        there = pl.ds(phase * half, half)
+        for columns in tiles:
+            slot_stream[there, columns] = jnp.dot(
+                place[there], stream[:, columns], preferred_element_type=jnp.float32
+            ).astype(jnp.bfloat16)
+
+    settle(arrived_share.at[:, 0], spread_recv.at[0])
     share_forward = pltpu.make_async_remote_copy(
         arrived_share.at[:, 0],
         arrived_share.at[:, 1],
@@ -542,19 +561,18 @@
         return dest, spot, pltpu.make_async_remote_copy(
             result.at[phase, block(spot)],
             fetched.at[block(me)],
-            back_send.at[step],
-            back_recv.at[me],
+            back_send.at[0],
+            back_recv.at[phase],
             device_id={"sp": dest},
         )
 
     own_back = pltpu.make_async_copy(
-        result.at[PHASES - 1, block(spot_of)], fetched.at[block(me)], back_recv.at[me]
+        result.at[PHASES - 1, block(spot_of)], fetched.at[block(me)], back_recv.at[PHASES - 1]
     )
 
     def meet_far():
-        for step in range(EARLY):
-            for copy in far[step]:
-                copy.wait_recv()
+        settle(early_recv, first_recv.at[0])
+        settle(pooled_recv, second_recv.at[0])
         for columns in tiles:
             far_mixed[:, columns] = jnp.dot(
                 pooled_recv[...], output_weight[:, columns], preferred_element_type=jnp.float32
@@ -580,36 +598,52 @@
     def return_phase(phase):
         lax.fori_loop(phase * per, (phase + 1) * per, start_back, 0)
 
-    def sent_near(step, carry):
-        dispatch(step)[1].wait_send()
-        return carry
-
-    def serve(turn, carry):
-        phase = in_order(turn, SERVE_ORDER)
-        pieces = [arrived_share[phase, core, spot] for core in range(2) for spot in range(per)]
-        pieces.append(jnp.zeros((LANES - 2 * per, LANES), jnp.float32))
-        turned = jnp.transpose(jnp.concatenate(pieces, axis=0))
-
-        def land(step, inner):
-            spot = lax.rem(spot_of + per - step, per)
-            settle(arrived.at[phase, block(spot)], recv_sem.at[phase * per + spot])
-            return inner
-
-        lax.fori_loop(jnp.where(phase == 0, EARLY, 0), per, land, 0)
-
-        @pl.when(phase == 0)
-        def _():
-            meet_far()
-
-        forward = pltpu.make_async_remote_copy(
+    def forward(phase):
+        return pltpu.make_async_remote_copy(
             arrived.at[phase, pl.ds(0, half)],
             arrived.at[phase, pl.ds(half, half)],
             forward_send.at[phase],
             forward_recv.at[phase],
             device_id={"tp": 1 - tp_rank},
         )
-        forward.start()
-        forward.wait()
+
+    def land(phase):
+        @pl.when(phase == 0)
+        def _():
+            if EARLY < per:
+                settle(arrived.at[0, pl.ds(0, half - EARLY * cap)], recv_sem.at[0])
+            meet_far()
+
+        @pl.when(phase != 0)
+        def _():
+            settle(arrived.at[phase, pl.ds(0, half)], recv_sem.at[phase])
+
+        forward(phase).start()
+
+    def swap(phase, index):
+        columns = tiles[index]
+        return pltpu.make_async_remote_copy(
+            outgoing.at[phase, :, columns],
+            incoming.at[phase, :, columns],
+            part_send.at[phase],
+            part_recv.at[phase],
+            device_id={"tp": 1 - tp_rank},
+        )
+
+    land(SERVE_ORDER[0])
+
+    def serve(turn, carry):
+        phase = in_order(turn, SERVE_ORDER)
+        later = in_order(turn, SERVE_ORDER[1:] + (0,))
+        pieces = [arrived_share[phase, core, spot] for core in range(2) for spot in range(per)]
+        pieces.append(jnp.zeros((LANES - 2 * per, LANES), jnp.float32))
+        turned = jnp.transpose(jnp.concatenate(pieces, axis=0))
+        forward(phase).wait()
+
+        @pl.when(turn == EAGER)
+        def _():
+            land(later)
+
         for expert in range(experts):
             given = arrived[phase]
             gate = jnp.dot(given, gates[expert], preferred_element_type=jnp.float32)
@@ -621,74 +655,69 @@
             )
             weighted = silu * upper * share
             hidden[:, expert * units : (expert + 1) * units] = weighted.astype(jnp.bfloat16)
-        for columns in tiles:
+        for index, columns in enumerate(tiles):
             product = jnp.dot(hidden[...], downs[:, columns], preferred_element_type=jnp.float32)
             kept[:, columns] = product[:half]
             outgoing[phase, :, columns] = product[half:].astype(jnp.bfloat16)
-        swap = pltpu.make_async_remote_copy(
-            outgoing.at[phase],
-            incoming.at[phase],
-            part_send.at[phase],
-            part_recv.at[phase],
-            device_id={"tp": 1 - tp_rank},
-        )
-        swap.start()
-        swap.wait()
-        result[phase] = (kept[...] + incoming[phase].astype(jnp.float32)).astype(jnp.bfloat16)
-
-        @pl.when(phase == 3)
+            swap(phase, index).start()
+
+        @pl.when((turn != EAGER) & (turn < PHASES - 1))
         def _():
-            return_phase(3)
-
-        @pl.when(phase == 2)
+            land(later)
+
+        settle(outgoing.at[phase], part_send.at[phase])
+        settle(incoming.at[phase], part_recv.at[phase])
+        for columns in tiles:
+            result[phase, :, columns] = (
+                kept[:, columns] + incoming[phase, :, columns].astype(jnp.float32)
+            ).astype(jnp.bfloat16)
+
+        @pl.when(turn == HOLDTURN)
         def _():
-            lax.fori_loop(per, 2 * per, sent_near, 0)
+            settle(send_ref.at[pl.ds(0, half)], send_sem.at[1])
             return_phase(0)
-            return_phase(2)
-
-        @pl.when(phase == 1)
+
+        @pl.when(phase != 0)
         def _():
-            return_phase(1)
+            return_phase(phase)
 
         return carry
 
     lax.fori_loop(0, PHASES, serve, 0)
     own_back.start()
 
-    def finish(step, carry):
-        settle(fetched.at[block(step)], back_recv.at[step])
-        dest, copy = dispatch(step)
-        _, _, home = back(step)
-        _, spread_out = share_copy(step)
-
-        @pl.when((dest != me) & (step >= EARLY) & (step // per != 1))
-        def _():
-            copy.wait_send()
-
-        @pl.when(dest != me)
-        def _():
-            home.wait_send()
-            spread_out.wait_send()
-
-        return carry
-
-    for first, second in far:
-        first.wait_send()
-        second.wait_send()
-    lax.fori_loop(0, count, finish, 0)
-    for columns in tiles:
-        mixed[:, columns] = jnp.dot(
-            pick[...], fetched[:, columns], preferred_element_type=jnp.float32
-        )
-
-    def update(index, carry):
-        here = pl.ds(pl.multiple_of(index * chunk, chunk), chunk)
-        out_ref[here] = (
-            stream[here].astype(jnp.float32) + scaled(mixed[here], final_gain)
+    for phase in FINISH_ORDER:
+        origin = other_plane(plane, phase)
+
+        def update(index, carry):
+            here = pl.ds(pl.multiple_of(origin * half + index * chunk, chunk), chunk)
+            slot_stream[here] = (
+                slot_stream[here].astype(jnp.float32)
+                + scaled(fetched[here].astype(jnp.float32), final_gain)
+            ).astype(jnp.bfloat16)
+            return carry
+
+        settle(fetched.at[pl.ds(0, half)], back_recv.at[phase])
+        lax.fori_loop(0, half // chunk, update, 0)
+    writes = []
+    for index, columns in enumerate(tiles):
+        final[:, columns] = jnp.dot(
+            pick[...], slot_stream[:, columns], preferred_element_type=jnp.float32
         ).astype(jnp.bfloat16)
-        return carry
-
-    lax.fori_loop(0, rows // chunk, update, 0)
+        writes.append(
+            pltpu.make_async_copy(
+                final.at[:, columns], out_hbm.at[:, columns], write_sem.at[index]
+            )
+        )
+        writes[-1].start()
+    settle(early_send, first_send.at[0])
+    settle(pooled_send, second_send.at[0])
+    settle(share_send.at[pl.ds(0, count - 1)], spread_send.at[0])
+    settle(fetched.at[pl.ds(0, (count - 1) * cap)], back_send.at[0])
+    for phase, blocks in ((0, per - EARLY), (2, per), (3, per - 1)):
+        settle(send_ref.at[pl.ds(0, blocks * cap)], send_sem.at[phase])
+    for write in writes:
+        write.wait()
 
 
 def local(
@@ -728,9 +757,11 @@
         in_specs=[whole, whole, outside, whole, whole, outside]
         + [whole] * 6
         + [outside] * 3,
-        out_specs=whole,
+        out_specs=outside,
         scratch_shapes=[
             vmem((length + 2 * reach, part), bf16),
+            vmem((2, reach // 2, LANES), bf16),
+            vmem((2, reach // 2, LANES), bf16),
             vmem((2, 1, reach), documents.dtype),
             vmem((docs, LANES), f32),
             vmem((count, docs, LANES), f32),
@@ -761,26 +792,29 @@
             vmem((PHASES, half, width), bf16),
             vmem((PHASES, half, width), bf16),
             vmem((PHASES, half, width), bf16),
+            vmem((slots, width), bf16),
+            vmem((rows, width), bf16),
             dma((6,)),
             dma((7,)),
-            dma((count,)),
-            dma((count,)),
+            dma((1,)),
+            dma((1,)),
             dma((4,)),
-            dma((count,)),
-            dma((count,)),
+            dma((1,)),
+            dma((1,)),
             dma((5,)),
-            dma((count,)),
-            dma((count,)),
             dma((PHASES,)),
             dma((PHASES,)),
             dma((PHASES,)),
             dma((PHASES,)),
-            dma((count,)),
-            dma((count,)),
-            dma((EARLY,)),
-            dma((EARLY,)),
-            dma((EARLY,)),
-            dma((EARLY,)),
+            dma((PHASES,)),
+            dma((PHASES,)),
+            dma((1,)),
+            dma((PHASES,)),
+            dma((1,)),
+            dma((1,)),
+            dma((1,)),
+            dma((1,)),
+            dma((4,)),
         ],
         compiler_params=pltpu.CompilerParams(
             collective_id=0, has_side_effects=True, vmem_limit_bytes=60 * 1024 * 1024

time: 116 us -> 114 us (0.983)
  Pallas kernels: 114 us -> 111 us
    pallas_call x1, Pallas kernels: 114 us -> 111 us  [local(): pl.pallas_call(functools.partial(layer_kernel, count, docs), out_shape=ja...]
where the time goes in v2:
time: 114 us
  Pallas kernels  111 us (97%)
  local copies, waits for them, and re-layouts  2.3 us (2%)
    pallas_call x1, Pallas kernels, local(): pl.pallas_call(functools.partial(layer_kernel, count, docs), out_shape=ja...  111 us
    unnamed x1, local copies, waits for them, and re-layouts  2.3 us

profile of v2, /device:TPU:0, one launch (start us, length us, event | category | flops | bytes accessed | tf_op | source)
XLA Modules:
  0.0 113.6 jit_solution(13677093804706544661)
XLA Ops:
  0.0 111.3 %shard_map.145 = bf16[256,2048]{1,0:T(8,128)(2,1)} custom-call(bf16[512,256]{1,0:T(8,128)(2,1)} %pool_ref.1, s32[2,1,256]{2,1,0:T(1,128)} %bitcast.6, bf16[256,2048]{1,0:T(8,128)(2,1)} %residual_hbm.1, bf16[8,64,64]{2,1,0:T(8,128)(2,1)} %weights_ref.1, bf16[512]{0:T(512)(128)(2,1)} %pool_gain_ref.1, bf16[512,2048]{1,0:T(8,128)(2,1)} %output_hbm.1, ...), custom_call_target="tpu_custom_call" | custom-call | tf_op jit(solution)/shard_map/pallas_call | solution.py:754
  111.3 2.3 %copy.17 = bf16[256,2048]{1,0:T(8,128)(2,1)} copy(bf16[256,2048]{1,0:T(8,128)(2,1)} %shard_map.145) | data formatting | bytes 2097152

commit v3 on v2

--- a/solution.py
+++ b/solution.py
@@ -484,7 +484,7 @@
     mixer_gain = mixer_gain_ref[...].astype(jnp.float32).reshape(1, -1)
     routed_gain = routed_gain_ref[...].astype(jnp.float32).reshape(1, -1)
     final_gain = final_gain_ref[...].astype(jnp.float32).reshape(1, -1)
-    chunk = 32
+    chunk = min(128, half)
 
     def normalise(index, carry):
         here = pl.ds(pl.multiple_of(index * chunk, chunk), chunk)

time: 114 us -> 111 us (0.974)
  Pallas kernels: 111 us -> 108 us
    pallas_call x1, Pallas kernels: 111 us -> 108 us  [local(): pl.pallas_call(functools.partial(layer_kernel, count, docs), out_shape=ja...]
where the time goes in v3:
time: 111 us
  Pallas kernels  108 us (97%)
  local copies, waits for them, and re-layouts  2.3 us (2%)
    pallas_call x1, Pallas kernels, local(): pl.pallas_call(functools.partial(layer_kernel, count, docs), out_shape=ja...  108 us
    unnamed x1, local copies, waits for them, and re-layouts  2.3 us

profile of v3, /device:TPU:0, one launch (start us, length us, event | category | flops | bytes accessed | tf_op | source)
XLA Modules:
  0.0 110.6 jit_solution(305608379405780603)
XLA Ops:
  0.0 108.3 %shard_map.145 = bf16[256,2048]{1,0:T(8,128)(2,1)} custom-call(bf16[512,256]{1,0:T(8,128)(2,1)} %pool_ref.1, s32[2,1,256]{2,1,0:T(1,128)} %bitcast.6, bf16[256,2048]{1,0:T(8,128)(2,1)} %residual_hbm.1, bf16[8,64,64]{2,1,0:T(8,128)(2,1)} %weights_ref.1, bf16[512]{0:T(512)(128)(2,1)} %pool_gain_ref.1, bf16[512,2048]{1,0:T(8,128)(2,1)} %output_hbm.1, ...), custom_call_target="tpu_custom_call" | custom-call | tf_op jit(solution)/shard_map/pallas_call | solution.py:754
  108.3 2.3 %copy.17 = bf16[256,2048]{1,0:T(8,128)(2,1)} copy(bf16[256,2048]{1,0:T(8,128)(2,1)} %shard_map.145) | data formatting | bytes 2097152
